TPU v7x, 512 devices: a whole 4x4x16 slice. The times are simulated.
512 devices in a mesh: ep: 32 (over z, core), tp: 16 (over y, x).
Axes of the slice: x: 4, y: 4, z: 16, core: 2. Of those that a mesh axis runs over, the one named last changes fastest.
Arguments:
- tokens: bfloat16 [4096, 1024], P('ep', 'tp'), may hold values from -6 to 6
- norm_gain: float32 [1024], replicated, may hold values from 0.1 to 1.9
- gate_weight: bfloat16 [32, 1024, 1024], P('ep', None, 'tp'), may hold values from -0.1875 to 0.1875
- up_weight: bfloat16 [32, 1024, 1024], P('ep', None, 'tp'), may hold values from -0.1875 to 0.1875
- down_weight: bfloat16 [32, 1024, 1024], P('ep', None, 'tp'), may hold values from -0.1875 to 0.1875
- expert_ids: int32 [4096, 4], P('ep'), may hold values from 0 to 31, all different within a row; in each aligned block of 128 rows (0 to 127, 128 to 255, ...) at most 32 rows name the same one
- route_weight: float32 [4096, 4], P('ep'), may hold values from 0.2 to 1
Outputs:
- combined: bfloat16 [4096, 1024], P('ep', 'tp')
Inputs may be any that keep to these rules, and one draw needn't show every extreme that they name: `expert_ids`: each token names 4 different experts; in each aligned block of 128 tokens no expert is named by more than 32 of them, and in some block one expert is named by exactly 32; every expert is named by some token.
All inputs are finite; a program needn't handle non-finite values.
Results may differ from a plain program's by a relative error of at most 0.0035.
Values may be sent and summed in bfloat16 or wider, within the bound.
No kernel may reach another device: no remote copies, remote signals or barrier semaphores. Data moves between devices by JAX's collectives and lax.ppermute only.
A program may use at most 64 MiB of HBM per device.

v0:
```python
import jax
import jax.numpy as jnp
from jax import lax
from jax.sharding import Mesh
from jax.sharding import PartitionSpec as P

TP = ("tp_0", "tp_1")


epsilon = 1e-06
swish_alpha = 1.702
clamp_limit = 7.0


def by_axis(shard, axes):
    for axis in axes:
        shard = lax.psum(shard, axis)
    return shard


def whole_of(shard, axes, dim):
    if not axes:
        return shard
    nearer = lax.all_gather(shard, axes[-1], axis=dim, tiled=True)
    return whole_of(nearer, axes[:-1], dim)


def taken_in(shard, axes, dim, take_in, carry):
    everything = jax.tree.map(lambda part: whole_of(part, axes, dim), shard)
    return take_in(carry, everything, jnp.int32(0))


def slot_numbers(flat_ids, expert_count):
    selector = (flat_ids[..., None] == jnp.arange(expert_count, dtype=jnp.int32)).astype(jnp.int32)
    before = jnp.cumsum(selector, axis=-2) - selector
    return jnp.sum(before * selector, axis=-1).astype(jnp.int32)


def by_expert(incoming, ep_count, local_experts):
    capacity = incoming.shape[1]
    width = incoming.shape[2]
    grouped = incoming.reshape(ep_count, local_experts, capacity, width)
    return jnp.transpose(grouped, (1, 0, 2, 3)).reshape(local_experts, ep_count * capacity, width)


def body(tokens, norm_gain, gate_weight, up_weight, down_weight, expert_ids, route_weight):
    tok_rows = expert_ids.shape[0]
    top_count = expert_ids.shape[1]
    local_experts = gate_weight.shape[0]
    ep_count = lax.axis_size("ep")
    expert_total = local_experts * ep_count
    capacity = 2 * tok_rows * top_count // expert_total
    column_width = tokens.shape[1]
    hidden_width = gate_weight.shape[2]
    out_width = down_weight.shape[2]
    flat_ids = expert_ids.reshape(-1).astype(jnp.int32)
    slot_index = slot_numbers(flat_ids, expert_total)
    owner_token = jnp.arange(tok_rows * top_count, dtype=jnp.int32) // top_count
    slot_table = (
        jnp.full((expert_total, capacity), tok_rows, jnp.int32)
        .at[flat_ids, slot_index]
        .set(owner_token)
    )
    full_width = norm_gain.shape[0]
    widened = tokens.astype(jnp.float32)
    square_sum = by_axis(jnp.sum(widened * widened, axis=1), TP)
    inverse = lax.rsqrt(square_sum / full_width + epsilon)
    gain_part = lax.dynamic_slice_in_dim(
        norm_gain, lax.axis_index(TP) * column_width, column_width, 0
    )
    normed = (widened * inverse[:, None] * gain_part.astype(jnp.float32)).astype(jnp.bfloat16)
    padded = jnp.concatenate([normed, jnp.zeros((1, column_width), jnp.bfloat16)], axis=0)
    outgoing = padded[slot_table.reshape(-1)].reshape(expert_total, capacity, column_width)
    incoming = lax.all_to_all(outgoing, "ep", split_axis=0, concat_axis=0, tiled=True)
    row_block = by_expert(incoming, ep_count, local_experts)
    empty = jnp.zeros((local_experts, ep_count * capacity, hidden_width), jnp.float32)

    def add_columns(totals, piece, start):
        gate_rows = lax.dynamic_slice_in_dim(gate_weight, start, piece.shape[2], 1)
        up_rows = lax.dynamic_slice_in_dim(up_weight, start, piece.shape[2], 1)
        gate_part = jnp.einsum("esd,edf->esf", piece, gate_rows, preferred_element_type=jnp.float32)
        up_part = jnp.einsum("esd,edf->esf", piece, up_rows, preferred_element_type=jnp.float32)
        return (totals[0] + gate_part, totals[1] + up_part)

    gate_pre, up_pre = taken_in(row_block, TP, 2, add_columns, (empty, empty))
    gate_pre = jnp.minimum(gate_pre, clamp_limit)
    up_pre = jnp.clip(up_pre, -clamp_limit, clamp_limit)
    hidden = ((up_pre + 1.0) * gate_pre * jax.nn.sigmoid(swish_alpha * gate_pre)).astype(
        jnp.bfloat16
    )
    empty_out = jnp.zeros((local_experts, ep_count * capacity, out_width), jnp.float32)

    def add_hidden(total, piece, start):
        down_rows = lax.dynamic_slice_in_dim(down_weight, start, piece.shape[2], 1)
        return total + jnp.einsum(
            "esf,efd->esd", piece, down_rows, preferred_element_type=jnp.float32
        )

    down_sum = taken_in(hidden, TP, 2, add_hidden, empty_out)
    expert_out = down_sum.astype(jnp.bfloat16).reshape(local_experts, ep_count, capacity, out_width)
    sendback = jnp.transpose(expert_out, (1, 0, 2, 3)).reshape(
        ep_count * local_experts, capacity, out_width
    )
    returned = lax.all_to_all(sendback, "ep", split_axis=0, concat_axis=0, tiled=True)
    flat_back = returned.reshape(expert_total * capacity, out_width)
    picked = (
        flat_back[flat_ids * capacity + slot_index]
        .reshape(tok_rows, top_count, out_width)
        .astype(jnp.float32)
    )
    combined = jnp.sum(picked * route_weight.astype(jnp.float32)[:, :, None], axis=1)
    return combined.astype(jnp.bfloat16)


def solution(mesh):
    split = Mesh(mesh.devices.reshape(mesh.shape["ep"], 4, 4), ("ep", "tp_0", "tp_1"))
    in_specs = (
        P("ep", TP),
        P(),
        P("ep", None, TP),
        P("ep", None, TP),
        P("ep", None, TP),
        P("ep", None),
        P("ep", None),
    )
    out_specs = P("ep", TP)
    return jax.shard_map(body, mesh=split, in_specs=in_specs, out_specs=out_specs, check_vma=False)
```

profile of v0, /device:TPU:1, one launch (start us, length us, event | category | flops | bytes accessed | tf_op | source)
XLA Modules:
  0.0 231.8 jit_solution(11236081657783373569)
XLA Ops:
  6.5 0.0 copy-start
  6.5 0.0 all-gather.5.cloned.1.call-start
  6.5 0.8 copy.36
  7.4 0.1 eq.29
  7.5 0.1 eq.25
  7.6 0.1 reshape.162
  7.7 0.7 fusion.30
  8.4 9.5 %psum.14 = f32[128]{0:T(128)S(1)} all-reduce(f32[128]{0:T(128)S(1)} %fusion.30), channel_id=1, replica_groups=mesh['ep'=32,'tp_0'=4,'tp_1'=4] {'tp_0'}, use_global_device_ids=true, to_apply=%region_1.2 | all-reduce | flops 128 | bytes 1024 | tf_op jit(solution)/shard_map/psum | solution.py:17
  18.0 8.5 %psum.15 = f32[128]{0:T(128)S(1)} all-reduce(f32[128]{0:T(128)S(1)} %psum.14), channel_id=1, replica_groups=mesh['ep'=32,'tp_0'=4,'tp_1'=4] {'tp_1'}, use_global_device_ids=true, to_apply=%region_2.3 | all-reduce | flops 128 | bytes 1024 | tf_op jit(solution)/shard_map/psum | solution.py:17
  26.5 0.8 dynamic_slice.3
  27.2 0.8 fusion.32
  28.0 0.1 copy.45
  28.2 1.2 reduce-window.6
  29.3 0.2 slice_reduce_fusion
  29.6 0.1 fusion.28
  29.7 25.1 %scatter_fusion = s32[32,32]{1,0:T(8,128)S(1)} fusion(s32[32,32]{1,0:T(8,128)S(1)} %broadcast_in_dim.2, s32[512]{0:T(512)S(1)} %bitcast.56, s32[512]{0:T(512)S(1)} %add_select_fusion), kind=kCustom, calls=%fused_computation.2 | custom fusion | bytes 10240 | tf_op jit(solution)/shard_map/scatter | solution.py:62
  54.9 0.1 reshape.164
  55.0 3.2 %gather_fusion = bf16[1024,64]{1,0:T(8,128)(2,1)S(1)} fusion(bf16[129,64]{1,0:T(8,128)(2,1)S(1)} %concatenate.6.clone, s32[1024]{0:T(1024)S(1)} %broadcast_clamp_fusion), kind=kCustom, calls=%fused_computation | custom fusion | bytes 266240 | tf_op jit(solution)/shard_map/gather | solution.py:73
  58.2 0.2 reshape.199
  58.4 35.8 %all_to_all.10 = bf16[32,2,1024]{2,1,0:T(2,128)(2,1)S(1)} all-to-all(bf16[32,2,1024]{2,1,0:T(2,128)(2,1)S(1)} %reshape.199), channel_id=1, replica_groups=mesh['ep'=32,'tp_0'=4,'tp_1'=4] {'ep'}, dimensions={0} | all-to-all | bytes 262144 | tf_op jit(solution)/shard_map/all_to_all | solution.py:74
  94.3 0.2 reshape.200
  94.5 0.0 copy-start.4
  94.5 0.1 copy.41
  94.6 10.6 %all_gather.12 = bf16[1,1024,256]{1,2,0:T(8,128)(2,1)} all-gather(bf16[1,1024,64]{1,2,0:T(8,128)(2,1)S(1)} %copy.41), channel_id=1, replica_groups=mesh['ep'=32,'tp_0'=4,'tp_1'=4] {'tp_1'}, dimensions={2}, use_global_device_ids=true | all-gather | bytes 655360 | tf_op jit(solution)/shard_map/all_gather | solution.py:24
  105.3 0.0 all-gather.5.cloned.1.call-update
  105.3 0.0 all-gather.7.cloned.1.call-start
  105.3 29.3 %all-gather.5.cloned.1.call-done = bf16[1,1024,1024]{1,2,0:T(8,128)(2,1)} async-done(((bf16[1,1024,256]{1,2,0:T(8,128)(2,1)}), bf16[1,1024,1024]{1,2,0:T(8,128)(2,1)}) %all-gather.5.cloned.1.call-update) | async-done | bytes 2097168 | tf_op jit(solution)/shard_map/all_gather | solution.py:24
  134.7 0.0 copy-done
  134.7 2.2 fusion.4
  136.9 0.0 copy-done.4
  136.9 0.0 copy-done.1
  136.9 0.0 copy-start.2
  136.9 0.5 fusion.19
  137.5 12.2 %all-gather = bf16[1024,256]{0,1:T(8,128)(2,1)} all-gather(bf16[1024,64]{0,1:T(8,128)(2,1)S(1)} %fusion.19), channel_id=2, replica_groups=mesh['ep'=32,'tp_0'=4,'tp_1'=4] {'tp_1'}, dimensions={1}, use_global_device_ids=true | all-gather | bytes 655360 | tf_op jit(solution)/shard_map/all_gather | solution.py:24
  149.6 0.0 all-gather.7.cloned.1.call-update
  149.6 40.4 %all-gather.7.cloned.1.call-done = bf16[1024,1024]{0,1:T(8,128)(2,1)} async-done(((bf16[1024,256]{0,1:T(8,128)(2,1)}), bf16[1024,1024]{0,1:T(8,128)(2,1)}) %all-gather.7.cloned.1.call-update) | async-done | bytes 2097168 | tf_op jit(solution)/shard_map/all_gather | solution.py:24
  190.0 0.0 copy-done.2
  190.0 2.1 convolution_convert_fusion
  192.1 0.2 copy.42
  192.2 0.8 reshape.201
  193.1 13.3 %all-to-all-start.1 = ((bf16[32,2,1024]{2,1,0:T(2,128)(2,1)}), bf16[32,2,1024]{2,1,0:T(2,128)(2,1)S(1)}, u32[]{:S(2)}, u32[]{:S(2)}) async-start(bf16[32,2,1024]{2,1,0:T(2,128)(2,1)} %reshape.201), calls=%async_computation.1 | async-start | bytes 262144 | tf_op jit(solution)/shard_map/all_to_all | solution.py:104
  206.3 0.0 copy-done.3
  206.4 0.1 copy.43
  206.5 15.9 %all-to-all-done.1 = bf16[32,2,1024]{2,1,0:T(2,128)(2,1)S(1)} async-done(((bf16[32,2,1024]{2,1,0:T(2,128)(2,1)}), bf16[32,2,1024]{2,1,0:T(2,128)(2,1)S(1)}, u32[]{:S(2)}, u32[]{:S(2)}) %all-to-all-start.1) | async-done | bytes 131104 | tf_op jit(solution)/shard_map/all_to_all | solution.py:104
  222.4 0.2 reshape.202
  222.6 1.3 gather_fusion.1
  223.9 0.3 fusion.22
  224.2 0.7 copy.44
  (13 shorter events, 0.1 us)
Async XLA Ops:
  6.5 128.1 %copy-start = (bf16[1,1024,64]{1,2,0:T(8,128)(2,1)S(1)}, bf16[1,1024,64]{1,2,0:T(8,128)(2,1)}, u32[]{:S(2)}) copy-start(bf16[1,1024,64]{1,2,0:T(8,128)(2,1)} %param.9) | copy-start | bytes 393220
  6.5 128.1 %all-gather.5.cloned.1.call-start = ((), (), s32[]{:S(2)}) async-start(), calls=%async_computation.2 | async-start | bytes 2621440 | tf_op jit(solution)/shard_map/all_gather | solution.py:24
  94.5 42.4 %copy-start.4 = (bf16[1,1024,64]{1,2,0:T(8,128)(2,1)S(1)}, bf16[1,1024,64]{1,2,0:T(8,128)(2,1)}, u32[]{:S(2)}) copy-start(bf16[1,1024,64]{1,2,0:T(8,128)(2,1)} %param.10) | copy-start | bytes 393220
  105.3 84.7 %all-gather.7.cloned.1.call-start = ((), (), s32[]{:S(2)}) async-start(), calls=%async_computation.3 | async-start | bytes 2621440 | tf_op jit(solution)/shard_map/all_gather | solution.py:24
  134.7 2.2 copy-start.1
  136.9 53.1 %copy-start.2 = (bf16[1,1024,64]{1,2,0:T(8,128)(2,1)S(1)}, bf16[1,1024,64]{1,2,0:T(8,128)(2,1)}, u32[]{:S(2)}) copy-start(bf16[1,1024,64]{1,2,0:T(8,128)(2,1)} %param.11) | copy-start | bytes 393220
  149.6 56.7 %copy-start.3 = (f32[128,4]{0,1:T(4,128)S(1)}, f32[128,4]{0,1:T(4,128)}, u32[]{:S(2)}) copy-start(f32[128,4]{0,1:T(4,128)} %param.13) | copy-start | bytes 6148
  193.1 29.3 %all-to-all-start.1 = ((bf16[32,2,1024]{2,1,0:T(2,128)(2,1)}), bf16[32,2,1024]{2,1,0:T(2,128)(2,1)S(1)}, u32[]{:S(2)}, u32[]{:S(2)}) async-start(bf16[32,2,1024]{2,1,0:T(2,128)(2,1)} %reshape.201), calls=%async_computation.1 | async-start | bytes 262144 | tf_op jit(solution)/shard_map/all_to_all | solution.py:104
Sparse Core Ops, SparseCore 0:
  105.4 29.1 all-gather.4
  149.8 40.1 all-gather.6
where the time goes:
time: 232 us
  waiting for transfers between devices  85.6 us (37%)
  blocking collectives  76.6 us (33%)
  local copies, waits for them, and re-layouts  34.6 us (15%)
  between operations  13.6 us (6%)
  starting transfers between devices  13.3 us (6%)
  matrix products  4.82 us (2%)
  other arithmetic  3.18 us (1%)
    all_gather x2, waiting for transfers between devices, whole_of(): nearer = lax.all_gather(shard, axes[-1], axis=dim, tiled=True)  69.7 us
    all_to_all x1, blocking collectives, body(): lax.all_to_all(outgoing, 'ep', split_axis=0, concat_axis=0, tiled=True)  35.8 us
    scatter x1, local copies, waits for them, and re-layouts, body(): slot_table = jnp.full((expert_total, capacity), tok_rows, jnp.int32).at[f...  25.1 us
    all_gather x2, blocking collectives, whole_of(): nearer = lax.all_gather(shard, axes[-1], axis=dim, tiled=True)  22.8 us
    psum x2, blocking collectives, by_axis(): shard = lax.psum(shard, axis)  18 us
    all_to_all x1, waiting for transfers between devices, body(): lax.all_to_all(sendback, 'ep', split_axis=0, concat_axis=0, tiled=True)  15.9 us
    all_to_all x1, starting transfers between devices, body(): lax.all_to_all(sendback, 'ep', split_axis=0, concat_axis=0, tiled=True)  13.3 us
  transfers between devices with their start and end apart: 3, of which 3 were waited for; matrix products, arithmetic and copies ran while one was open for 0% of the time, Pallas kernels for 0%

commit v1 on v0

v1 whole, which is shorter than its diff:
```python
import jax
import jax.numpy as jnp
from jax import lax
from jax.sharding import Mesh
from jax.sharding import PartitionSpec as P

EP, TY, TX = "ep", "ty", "tx"
TP = (TY, TX)
EPSILON = 1e-06
ALPHA = 1.702
LIMIT = 7.0
BF16, F32 = jnp.bfloat16, jnp.float32


def routed_to(expert_ids, expert_count):
    experts = jnp.arange(expert_count, dtype=jnp.int32)
    picks = expert_ids[:, :, None] == experts
    named = jnp.any(picks, axis=1)
    tok_rows = expert_ids.shape[0]
    earlier = jnp.arange(tok_rows)[:, None] > jnp.arange(tok_rows)[None, :]
    before = jnp.dot(earlier.astype(BF16), named.astype(BF16), preferred_element_type=F32)
    return jnp.sum(jnp.where(picks, before[:, None, :], 0.0), axis=2).astype(jnp.int32)


def body(tokens, norm_gain, gate_weight, up_weight, down_weight, expert_ids, route_weight):
    tok_rows, top = expert_ids.shape
    width = tokens.shape[1]
    full = norm_gain.shape[0]
    ep, ny, nx = lax.axis_size(EP), lax.axis_size(TY), lax.axis_size(TX)
    tp = ny * nx
    units = gate_weight.shape[2]
    half = tok_rows * top // ep
    group = ep // nx * half

    gate_up = jnp.concatenate([gate_weight[0], up_weight[0]], axis=1)
    gate_up = lax.all_to_all(
        jnp.broadcast_to(gate_up, (nx,) + gate_up.shape), TX, 0, 0, tiled=True
    )
    mine = nx * units
    down = down_weight[0].reshape(ny, 2, mine // 2, width)
    down = jnp.transpose(down, (0, 2, 1, 3)).reshape(ny, 1, mine // 2, 2 * width)
    down = jnp.broadcast_to(down, (ny, nx, mine // 2, 2 * width)).reshape(tp, mine // 2, 2 * width)
    down = lax.all_to_all(down, TP, 0, 0, tiled=True)

    slot = routed_to(expert_ids, ep)
    place = expert_ids * half + slot % half
    high = slot // half
    lanes = jnp.arange(ep * half, dtype=jnp.int32)
    hits = place[:, :, None] == lanes
    sel = [jnp.any(hits & (high == h)[:, :, None], axis=1).astype(BF16) for h in (0, 1)]
    sent = jnp.concatenate(
        [jnp.einsum("tp,tf->pf", s, tokens, preferred_element_type=F32) for s in sel], axis=1
    ).astype(BF16)
    got = lax.all_to_all(sent.reshape(ep, half, 2 * width), EP, 0, 0, tiled=True)

    got = got.reshape(1, nx, group, 2 * width)
    got = jnp.broadcast_to(got, (ny, nx, group, 2 * width)).reshape(tp, group, 2 * width)
    got = lax.all_to_all(got, TP, 0, 0, tiled=True)
    rows = jnp.transpose(got.reshape(tp, group, 2, width), (2, 1, 0, 3)).reshape(2 * group, full)
    rows = rows.astype(F32)
    inverse = lax.rsqrt(jnp.mean(rows * rows, axis=1, keepdims=True) + EPSILON)
    normed = (rows * inverse * norm_gain.astype(F32)).astype(BF16)
    gate_pre = jnp.einsum("rd,xdf->rxf", normed, gate_up[:, :, :units], preferred_element_type=F32)
    up_pre = jnp.einsum("rd,xdf->rxf", normed, gate_up[:, :, units:], preferred_element_type=F32)
    gate_pre = jnp.minimum(gate_pre, LIMIT)
    up_pre = jnp.clip(up_pre, -LIMIT, LIMIT)
    hidden = ((up_pre + 1.0) * gate_pre * jax.nn.sigmoid(ALPHA * gate_pre)).astype(BF16)
    hidden = hidden.reshape(2 * group, mine)
    w_down = jnp.transpose(down.reshape(tp, mine // 2, 2, width), (2, 1, 0, 3)).reshape(mine, full)
    part = jnp.dot(hidden, w_down, preferred_element_type=F32)
    part = jnp.transpose(part.reshape(2, group, tp, width), (2, 1, 0, 3))
    part = lax.all_to_all(part.reshape(tp, group, 2 * width), TP, 0, 0, tiled=True)
    out = jnp.sum(part.reshape(ny, nx * group, 2 * width), axis=0).astype(BF16)

    back = lax.all_to_all(out.reshape(ep, half, 2 * width), EP, 0, 0, tiled=True)
    back = back.reshape(ep * half, 2 * width)
    total = jnp.zeros((tok_rows, width), F32)
    for h in (0, 1):
        mix = jnp.sum(
            jnp.where(hits & (high == h)[:, :, None], route_weight[:, :, None], 0.0), axis=1
        )
        mix_hi = mix.astype(BF16)
        mix_lo = (mix - mix_hi.astype(F32)).astype(BF16)
        piece = back[:, h * width : (h + 1) * width]
        total = total + jnp.dot(mix_hi, piece, preferred_element_type=F32)
        total = total + jnp.dot(mix_lo, piece, preferred_element_type=F32)
    return total.astype(BF16)


def solution(mesh):
    devices = mesh.devices.reshape(mesh.shape["ep"], 4, 4)
    split = Mesh(devices, (EP, TY, TX))
    in_specs = (
        P(EP, TP),
        P(),
        P(EP, None, TP),
        P(EP, None, TP),
        P(EP, None, TP),
        P(EP, None),
        P(EP, None),
    )
    return jax.shard_map(
        body, mesh=split, in_specs=in_specs, out_specs=P(EP, TP), check_vma=False
    )
```

time: 232 us -> 136 us (0.59)
  blocking collectives: 76.6 us -> 19.1 us
  starting transfers between devices: 13.3 us -> 41.5 us
  local copies, waits for them, and re-layouts: 34.6 us -> 7.05 us
  waiting for transfers between devices: 85.6 us -> 61.6 us
  between operations: 13.6 us -> 0.29 us
    all_gather x2 -> x0, waiting for transfers between devices: 69.7 us -> none  [whole_of(): nearer = lax.all_gather(shard, axes[-1], axis=dim, tiled=True)]
    all_to_all x1 -> x5, waiting for transfers between devices: 15.9 us -> 61.6 us  [the longest x1 16 us: body(): lax.all_to_all(sent.reshape(ep, half, 2 * width), EP, 0, 0, tiled=True)]
    all_to_all x1 -> x5, starting transfers between devices: 13.3 us -> 41.5 us  [the longest x1 19.4 us: body(): lax.all_to_all(sent.reshape(ep, half, 2 * width), EP, 0, 0, tiled=True)]
    scatter x1 -> x0, local copies, waits for them, and re-layouts: 25.1 us -> none  [body(): slot_table = jnp.full((expert_total, capacity), tok_rows, jnp.int32).at[f...]
    all_gather x2 -> x0, blocking collectives: 22.8 us -> none  [whole_of(): nearer = lax.all_gather(shard, axes[-1], axis=dim, tiled=True)]
    psum x2 -> x0, blocking collectives: 18 us -> none  [by_axis(): shard = lax.psum(shard, axis)]
    all_to_all x1, blocking collectives: 35.8 us -> 19.1 us  [body(): lax.all_to_all(part.reshape(tp, group, 2 * width), TP, 0, 0, tiled=True)]
    gather x2 -> x0, local copies, waits for them, and re-layouts: 4.55 us -> none  [the longest x1 3.21 us: body(): padded[slot_table.reshape(-1)].reshape(expert_total, capacity, column_width)]
  transfers between devices with their start and end apart: 3 -> 5, of which waited for: 3 -> 5; matrix products, arithmetic and copies ran while one was open for 0% -> 2% of each run, Pallas kernels for 0% -> 0%
where the time goes in v1:
time: 136 us; the launch traced here: 135 us
  waiting for transfers between devices  61.6 us (45%)
  starting transfers between devices  41.5 us (31%)
  blocking collectives  19.1 us (14%)
  local copies, waits for them, and re-layouts  7.05 us (5%)
  matrix products  3.21 us (2%)
  other arithmetic  2.6 us (2%)
    all_to_all x1, starting transfers between devices, body(): lax.all_to_all(sent.reshape(ep, half, 2 * width), EP, 0, 0, tiled=True)  19.4 us
    all_to_all x1, blocking collectives, body(): lax.all_to_all(part.reshape(tp, group, 2 * width), TP, 0, 0, tiled=True)  19.1 us
    all_to_all x1, waiting for transfers between devices, body(): lax.all_to_all(sent.reshape(ep, half, 2 * width), EP, 0, 0, tiled=True)  16 us
    all_to_all x1, waiting for transfers between devices, body(): lax.all_to_all(out.reshape(ep, half, 2 * width), EP, 0, 0, tiled=True)  15.6 us
    all_to_all x1, waiting for transfers between devices, body(): lax.all_to_all(jnp.broadcast_to(gate_up, (nx,) + gate_up.shape), TX, 0, 0...  14.3 us
    all_to_all x1, waiting for transfers between devices, body(): got = lax.all_to_all(got, TP, 0, 0, tiled=True)  8.89 us
    all_to_all x1, starting transfers between devices, body(): down = lax.all_to_all(down, TP, 0, 0, tiled=True)  7.71 us
    all_to_all x1, starting transfers between devices, body(): lax.all_to_all(out.reshape(ep, half, 2 * width), EP, 0, 0, tiled=True)  7.29 us
  transfers between devices with their start and end apart: 5, of which 5 were waited for; matrix products, arithmetic and copies ran while one was open for 2% of the time, Pallas kernels for 0%

profile of v1, /device:TPU:1, one launch (start us, length us, event | category | flops | bytes accessed | tf_op | source)
XLA Modules:
  0.0 135.4 jit_solution(6288988435778414924)
XLA Ops:
  0.0 0.0 copy-start
  0.0 1.0 reshape_squeeze.3
  1.0 0.9 broadcast_in_dim.68
  1.9 7.7 %all-to-all-start.3 = ((bf16[16,128,128]{1,2,0:T(8,128)(2,1)}), bf16[16,128,128]{1,2,0:T(8,128)(2,1)S(1)}, u32[]{:S(2)}, u32[]{:S(2)}) async-start(bf16[16,128,128]{1,2,0:T(8,128)(2,1)} %bitcast.23), calls=%async_computation.3 | async-start | bytes 1048576 | tf_op jit(solution)/shard_map/all_to_all | solution.py:43
  9.6 0.0 copy-done.3
  9.7 0.1 fusion.18
  9.9 0.3 fusion.5
  10.2 0.2 copy.54
  10.4 0.2 copy.53
  10.6 0.0 copy-done
  10.6 0.2 convolution_convert_fusion
  10.7 0.2 convolution_convert_fusion.1
  10.9 0.8 pad_maximum_fusion.1
  11.7 6.9 %all-to-all-done.3 = bf16[16,128,128]{1,2,0:T(8,128)(2,1)S(1)} async-done(((bf16[16,128,128]{1,2,0:T(8,128)(2,1)}), bf16[16,128,128]{1,2,0:T(8,128)(2,1)S(1)}, u32[]{:S(2)}, u32[]{:S(2)}) %all-to-all-start.3) | async-done | bytes 524320 | tf_op jit(solution)/shard_map/all_to_all | solution.py:43
  18.6 19.4 %all-to-all-start = ((bf16[32,16,128]{2,1,0:T(8,128)(2,1)}), bf16[32,16,128]{2,1,0:T(8,128)(2,1)S(1)}, u32[]{:S(2)}, u32[]{:S(2)}) async-start(bf16[32,16,128]{2,1,0:T(8,128)(2,1)} %pad_maximum_fusion.1), calls=%async_computation | async-start | bytes 262144 | tf_op jit(solution)/shard_map/all_to_all | solution.py:54
  38.0 0.0 copy-done.1
  38.0 0.0 copy-done.2
  38.1 16.0 %all-to-all-done = bf16[32,16,128]{2,1,0:T(8,128)(2,1)S(1)} async-done(((bf16[32,16,128]{2,1,0:T(8,128)(2,1)}), bf16[32,16,128]{2,1,0:T(8,128)(2,1)S(1)}, u32[]{:S(2)}, u32[]{:S(2)}) %all-to-all-start) | async-done | bytes 131104 | tf_op jit(solution)/shard_map/all_to_all | solution.py:54
  54.0 1.1 broadcast_in_dim.66
  55.2 3.5 %all-to-all-start.2 = ((bf16[4,1024,128]{1,2,0:T(8,128)(2,1)}), bf16[4,1024,128]{1,2,0:T(8,128)(2,1)S(1)}, u32[]{:S(2)}, u32[]{:S(2)}) async-start(bf16[4,1024,128]{1,2,0:T(8,128)(2,1)} %broadcast_in_dim.66), calls=%async_computation.2 | async-start | bytes 2097152 | tf_op jit(solution)/shard_map/all_to_all | solution.py:36
  58.7 0.1 copy.55
  58.8 14.3 %all-to-all-done.2 = bf16[4,1024,128]{1,2,0:T(8,128)(2,1)S(1)} async-done(((bf16[4,1024,128]{1,2,0:T(8,128)(2,1)}), bf16[4,1024,128]{1,2,0:T(8,128)(2,1)S(1)}, u32[]{:S(2)}, u32[]{:S(2)}) %all-to-all-start.2) | async-done | bytes 1048608 | tf_op jit(solution)/shard_map/all_to_all | solution.py:36
  73.1 0.9 broadcast_in_dim.65
  74.0 3.6 %all-to-all-start.1 = ((bf16[16,128,128]{1,2,0:T(8,128)(2,1)}), bf16[16,128,128]{1,2,0:T(8,128)(2,1)S(1)}, u32[]{:S(2)}, u32[]{:S(2)}) async-start(bf16[16,128,128]{1,2,0:T(8,128)(2,1)} %bitcast.6), calls=%async_computation.1 | async-start | bytes 1048576 | tf_op jit(solution)/shard_map/all_to_all | solution.py:58
  77.6 0.5 copy.60
  78.1 0.1 copy.77
  78.2 0.1 fusion.27
  78.3 8.9 %all-to-all-done.1 = bf16[16,128,128]{1,2,0:T(8,128)(2,1)S(1)} async-done(((bf16[16,128,128]{1,2,0:T(8,128)(2,1)}), bf16[16,128,128]{1,2,0:T(8,128)(2,1)S(1)}, u32[]{:S(2)}, u32[]{:S(2)}) %all-to-all-start.1) | async-done | bytes 524320 | tf_op jit(solution)/shard_map/all_to_all | solution.py:58
  87.2 0.1 convert_element_type.86
  87.3 0.8 copy.56
  88.1 0.1 multiply_reduce_fusion
  88.2 0.0 copy-start.4
  88.3 0.7 copy-done.4
  88.9 0.4 fusion.23
  89.3 0.4 fusion.25
  89.8 0.1 multiply_convert_fusion
  89.9 0.3 convolution_bitcast_fusion
  90.2 0.1 copy.62
  90.3 19.1 %all_to_all.30 = f32[16,128,128]{1,2,0:T(8,128)S(1)} all-to-all(f32[16,128,128]{1,2,0:T(8,128)S(1)} %bitcast.81), channel_id=1, replica_groups=mesh['ep'=32,'ty'=4,'tx'=4] {'ty','tx'}, dimensions={0} | all-to-all | bytes 2097152 | tf_op jit(solution)/shard_map/all_to_all | solution.py:72
  109.4 0.3 copy.63
  109.8 0.7 bitcast_reduce_fusion
  110.5 7.3 %all-to-all-start.5 = ((bf16[32,16,128]{2,1,0:T(8,128)(2,1)}), bf16[32,16,128]{2,1,0:T(8,128)(2,1)S(1)}, u32[]{:S(2)}, u32[]{:S(2)}) async-start(bf16[32,16,128]{2,1,0:T(8,128)(2,1)} %bitcast.32), calls=%async_computation.5 | async-start | bytes 262144 | tf_op jit(solution)/shard_map/all_to_all | solution.py:75
  117.8 0.4 select_reduce_fusion
  118.2 15.6 %all-to-all-done.5 = bf16[32,16,128]{2,1,0:T(8,128)(2,1)S(1)} async-done(((bf16[32,16,128]{2,1,0:T(8,128)(2,1)}), bf16[32,16,128]{2,1,0:T(8,128)(2,1)S(1)}, u32[]{:S(2)}, u32[]{:S(2)}) %all-to-all-start.5) | async-done | bytes 131104 | tf_op jit(solution)/shard_map/all_to_all | solution.py:75
  133.8 0.2 fusion.11
  134.0 0.2 convolution_add_fusion.2
  134.2 0.3 convolution_add_fusion.1
  134.5 0.9 fusion
  (15 shorter events, 0.2 us)
Async XLA Ops:
  0.0 10.6 %copy-start = (bf16[128,64]{0,1:T(8,128)(2,1)S(1)}, bf16[128,64]{0,1:T(8,128)(2,1)}, u32[]{:S(2)}) copy-start(bf16[128,64]{0,1:T(8,128)(2,1)} %param.7) | copy-start | bytes 49156
  1.9 7.7 %copy-start.3 = (s32[128,4]{0,1:T(4,128)S(1)}, s32[128,4]{0,1:T(4,128)}, u32[]{:S(2)}) copy-start(s32[128,4]{0,1:T(4,128)} %param.12) | copy-start | bytes 6148
  1.9 16.7 %all-to-all-start.3 = ((bf16[16,128,128]{1,2,0:T(8,128)(2,1)}), bf16[16,128,128]{1,2,0:T(8,128)(2,1)S(1)}, u32[]{:S(2)}, u32[]{:S(2)}) async-start(bf16[16,128,128]{1,2,0:T(8,128)(2,1)} %bitcast.23), calls=%async_computation.3 | async-start | bytes 1048576 | tf_op jit(solution)/shard_map/all_to_all | solution.py:43
  11.7 26.3 %copy-start.1 = (bf16[1,1024,64]{1,2,0:T(8,128)(2,1)S(1)}, bf16[1,1024,64]{1,2,0:T(8,128)(2,1)}, u32[]{:S(2)}) copy-start(bf16[1,1024,64]{1,2,0:T(8,128)(2,1)} %param.10) | copy-start | bytes 393220
  11.7 26.3 %copy-start.2 = (bf16[1,1024,64]{1,2,0:T(8,128)(2,1)S(1)}, bf16[1,1024,64]{1,2,0:T(8,128)(2,1)}, u32[]{:S(2)}) copy-start(bf16[1,1024,64]{1,2,0:T(8,128)(2,1)} %param.9) | copy-start | bytes 393220
  18.6 35.4 %all-to-all-start = ((bf16[32,16,128]{2,1,0:T(8,128)(2,1)}), bf16[32,16,128]{2,1,0:T(8,128)(2,1)S(1)}, u32[]{:S(2)}, u32[]{:S(2)}) async-start(bf16[32,16,128]{2,1,0:T(8,128)(2,1)} %pad_maximum_fusion.1), calls=%async_computation | async-start | bytes 262144 | tf_op jit(solution)/shard_map/all_to_all | solution.py:54
  55.2 17.9 %all-to-all-start.2 = ((bf16[4,1024,128]{1,2,0:T(8,128)(2,1)}), bf16[4,1024,128]{1,2,0:T(8,128)(2,1)S(1)}, u32[]{:S(2)}, u32[]{:S(2)}) async-start(bf16[4,1024,128]{1,2,0:T(8,128)(2,1)} %broadcast_in_dim.66), calls=%async_computation.2 | async-start | bytes 2097152 | tf_op jit(solution)/shard_map/all_to_all | solution.py:36
  74.0 13.2 %all-to-all-start.1 = ((bf16[16,128,128]{1,2,0:T(8,128)(2,1)}), bf16[16,128,128]{1,2,0:T(8,128)(2,1)S(1)}, u32[]{:S(2)}, u32[]{:S(2)}) async-start(bf16[16,128,128]{1,2,0:T(8,128)(2,1)} %bitcast.6), calls=%async_computation.1 | async-start | bytes 1048576 | tf_op jit(solution)/shard_map/all_to_all | solution.py:58
  88.2 0.7 copy-start.4
  110.4 7.3 %copy-start.5 = (f32[128,4]{0,1:T(4,128)S(1)}, f32[128,4]{0,1:T(4,128)}, u32[]{:S(2)}) copy-start(f32[128,4]{0,1:T(4,128)} %param.13) | copy-start | bytes 6148
  110.5 23.3 %all-to-all-start.5 = ((bf16[32,16,128]{2,1,0:T(8,128)(2,1)}), bf16[32,16,128]{2,1,0:T(8,128)(2,1)S(1)}, u32[]{:S(2)}, u32[]{:S(2)}) async-start(bf16[32,16,128]{2,1,0:T(8,128)(2,1)} %bitcast.32), calls=%async_computation.5 | async-start | bytes 262144 | tf_op jit(solution)/shard_map/all_to_all | solution.py:75

commit v2 on v1

--- a/solution.py
+++ b/solution.py
@@ -22,6 +22,17 @@
     return jnp.sum(jnp.where(picks, before[:, None, :], 0.0), axis=2).astype(jnp.int32)
 
 
+def gathered(shard, axis):
+    count = lax.axis_size(axis)
+    me = lax.axis_index(axis)
+    whole = jnp.zeros((count,) + shard.shape, shard.dtype)
+    whole = lax.dynamic_update_slice_in_dim(whole, shard[None], me, 0)
+    for hop in range(1, count):
+        piece = lax.ppermute(shard, axis, [(i, (i + hop) % count) for i in range(count)])
+        whole = lax.dynamic_update_slice_in_dim(whole, piece[None], (me - hop) % count, 0)
+    return whole
+
+
 def body(tokens, norm_gain, gate_weight, up_weight, down_weight, expert_ids, route_weight):
     tok_rows, top = expert_ids.shape
     width = tokens.shape[1]
@@ -31,16 +42,12 @@
     units = gate_weight.shape[2]
     half = tok_rows * top // ep
     group = ep // nx * half
+    mine = nx * units
 
-    gate_up = jnp.concatenate([gate_weight[0], up_weight[0]], axis=1)
-    gate_up = lax.all_to_all(
-        jnp.broadcast_to(gate_up, (nx,) + gate_up.shape), TX, 0, 0, tiled=True
-    )
-    mine = nx * units
-    down = down_weight[0].reshape(ny, 2, mine // 2, width)
-    down = jnp.transpose(down, (0, 2, 1, 3)).reshape(ny, 1, mine // 2, 2 * width)
-    down = jnp.broadcast_to(down, (ny, nx, mine // 2, 2 * width)).reshape(tp, mine // 2, 2 * width)
-    down = lax.all_to_all(down, TP, 0, 0, tiled=True)
+    with jax.named_scope("weights"):
+        shard = jnp.stack([w[0].T for w in (gate_weight, up_weight, down_weight)])
+        weights = gathered(shard, TX)
+    w_gate, w_up, w_down = (weights[:, i].reshape(mine, full) for i in range(3))
 
     slot = routed_to(expert_ids, ep)
     place = expert_ids * half + slot % half
@@ -60,30 +67,30 @@
     rows = rows.astype(F32)
     inverse = lax.rsqrt(jnp.mean(rows * rows, axis=1, keepdims=True) + EPSILON)
     normed = (rows * inverse * norm_gain.astype(F32)).astype(BF16)
-    gate_pre = jnp.einsum("rd,xdf->rxf", normed, gate_up[:, :, :units], preferred_element_type=F32)
-    up_pre = jnp.einsum("rd,xdf->rxf", normed, gate_up[:, :, units:], preferred_element_type=F32)
+    gate_pre = jnp.einsum("fd,rd->fr", w_gate, normed, preferred_element_type=F32)
+    up_pre = jnp.einsum("fd,rd->fr", w_up, normed, preferred_element_type=F32)
     gate_pre = jnp.minimum(gate_pre, LIMIT)
     up_pre = jnp.clip(up_pre, -LIMIT, LIMIT)
     hidden = ((up_pre + 1.0) * gate_pre * jax.nn.sigmoid(ALPHA * gate_pre)).astype(BF16)
-    hidden = hidden.reshape(2 * group, mine)
-    w_down = jnp.transpose(down.reshape(tp, mine // 2, 2, width), (2, 1, 0, 3)).reshape(mine, full)
-    part = jnp.dot(hidden, w_down, preferred_element_type=F32)
-    part = jnp.transpose(part.reshape(2, group, tp, width), (2, 1, 0, 3))
-    part = lax.all_to_all(part.reshape(tp, group, 2 * width), TP, 0, 0, tiled=True)
-    out = jnp.sum(part.reshape(ny, nx * group, 2 * width), axis=0).astype(BF16)
 
-    back = lax.all_to_all(out.reshape(ep, half, 2 * width), EP, 0, 0, tiled=True)
-    back = back.reshape(ep * half, 2 * width)
+    hidden = jnp.broadcast_to(hidden, (ny,) + hidden.shape)
+    hidden = lax.all_to_all(hidden, TY, 0, 0, tiled=True).reshape(full, 2 * group)
+    out = jnp.dot(w_down, hidden, preferred_element_type=F32).astype(BF16)
+    out = lax.all_to_all(out.reshape(nx, width, 2 * group), TX, 0, 0, tiled=True)
+    out = out.reshape(nx, width, 2, ep // nx, half)
+    out = jnp.transpose(out, (0, 3, 4, 2, 1)).reshape(ep, half, 2 * width)
+
+    back = lax.all_to_all(out, EP, 0, 0, tiled=True).reshape(ep * half, 2 * width)
     total = jnp.zeros((tok_rows, width), F32)
     for h in (0, 1):
         mix = jnp.sum(
             jnp.where(hits & (high == h)[:, :, None], route_weight[:, :, None], 0.0), axis=1
         )
-        mix_hi = mix.astype(BF16)
-        mix_lo = (mix - mix_hi.astype(F32)).astype(BF16)
+        first = lax.reduce_precision(mix, 8, 7)
+        rest = lax.reduce_precision(mix - first, 8, 7)
         piece = back[:, h * width : (h + 1) * width]
-        total = total + jnp.dot(mix_hi, piece, preferred_element_type=F32)
-        total = total + jnp.dot(mix_lo, piece, preferred_element_type=F32)
+        for part in (first, rest):
+            total = total + jnp.dot(part.astype(BF16), piece, preferred_element_type=F32)
     return total.astype(BF16)
 
 

time: 136 us -> 113 us (0.83)
  waiting for transfers between devices: 61.6 us -> 40.3 us
  other arithmetic: 2.6 us -> 5.13 us
  starting transfers between devices: 41.5 us -> 39.4 us
  local copies, waits for them, and re-layouts: 7.05 us -> 5.5 us
    all_to_all x3 -> x1, waiting for transfers between devices: 36.8 us -> 15.8 us  [body(): lax.all_to_all(out, EP, 0, 0, tiled=True).reshape(ep * half, 2 * width)]
    all_to_all x3 -> x1, starting transfers between devices: 18.5 us -> 6.78 us  [body(): lax.all_to_all(out, EP, 0, 0, tiled=True).reshape(ep * half, 2 * width)]
    ppermute x0 -> x3, starting transfers between devices: none -> 11.5 us  [gathered(): lax.ppermute(shard, axis, [(i, (i + hop) % count) for i in range(count)])]
    all_to_all x1, starting transfers between devices: 19.4 us -> 16.8 us  [body(): lax.all_to_all(sent.reshape(ep, half, 2 * width), EP, 0, 0, tiled=True)]
    broadcast_in_dim x2, local copies, waits for them, and re-layouts: 2.01 us -> 0.22 us  [the longest x1 0.18 us: gathered(): whole = jnp.zeros((count,) + shard.shape, shard.dtype)]
    all_to_all x1, waiting for transfers between devices: 16 us -> 14.5 us  [body(): lax.all_to_all(sent.reshape(ep, half, 2 * width), EP, 0, 0, tiled=True)]
    all_to_all x1 -> x2, blocking collectives: 19.1 us -> 18.6 us  [the longest x1 10.5 us: body(): lax.all_to_all(hidden, TY, 0, 0, tiled=True).reshape(full, 2 * group)]
  transfers between devices with their start and end apart: 5 -> 6, of which waited for: 5 -> 3; matrix products, arithmetic and copies ran while one was open for 2% -> 7% of each run, Pallas kernels for 0% -> 0%
where the time goes in v2:
time: 113 us; the launch traced here: 112 us
  waiting for transfers between devices  40.3 us (36%)
  starting transfers between devices  39.4 us (35%)
  blocking collectives  18.6 us (16%)
  local copies, waits for them, and re-layouts  5.5 us (5%)
  other arithmetic  5.13 us (5%)
  matrix products  3.01 us (3%)
    all_to_all x1, starting transfers between devices, body(): lax.all_to_all(sent.reshape(ep, half, 2 * width), EP, 0, 0, tiled=True)  16.8 us
    all_to_all x1, waiting for transfers between devices, body(): lax.all_to_all(out, EP, 0, 0, tiled=True).reshape(ep * half, 2 * width)  15.8 us
    all_to_all x1, waiting for transfers between devices, body(): lax.all_to_all(sent.reshape(ep, half, 2 * width), EP, 0, 0, tiled=True)  14.5 us
    ppermute x3, starting transfers between devices, gathered(): lax.ppermute(shard, axis, [(i, (i + hop) % count) for i in range(count)])  11.5 us
    all_to_all x1, blocking collectives, body(): lax.all_to_all(hidden, TY, 0, 0, tiled=True).reshape(full, 2 * group)  10.5 us
    all_to_all x1, waiting for transfers between devices, body(): got = lax.all_to_all(got, TP, 0, 0, tiled=True)  10 us
    all_to_all x1, blocking collectives, body(): lax.all_to_all(out.reshape(nx, width, 2 * group), TX, 0, 0, tiled=True)  8.03 us
    all_to_all x1, starting transfers between devices, body(): lax.all_to_all(out, EP, 0, 0, tiled=True).reshape(ep * half, 2 * width)  6.78 us
  transfers between devices with their start and end apart: 6, of which 3 were waited for; matrix products, arithmetic and copies ran while one was open for 7% of the time, Pallas kernels for 0%

profile of v2, /device:TPU:1, one launch (start us, length us, event | category | flops | bytes accessed | tf_op | source)
XLA Modules:
  0.0 112.3 jit_solution(18389984339430377884)
XLA Ops:
  0.0 1.1 pad_maximum_fusion
  1.1 0.0 copy-start.2
  1.1 0.0 copy-start.3
  1.1 0.0 copy-start.4
  1.1 4.1 %collective-permute-start = (bf16[3,64,1024]{2,1,0:T(8,128)(2,1)S(1)}, bf16[3,64,1024]{2,1,0:T(8,128)(2,1)}, u32[]{:S(2)}, u32[]{:S(2)}) collective-permute-start(bf16[3,64,1024]{2,1,0:T(8,128)(2,1)S(1)} %pad_maximum_fusion), channel_id=1, source_target_pairs={{0,1},{1,2},{2,3},{3,0},{4,5},{5,6},{6,7},{7,4},{8,9},{9,10},{10,1... | collective-permute-start | bytes 1179656 | tf_op jit(solution)/shard_map/weights/ppermute | solution.py:31
  5.2 4.4 %collective-permute-start.1 = (bf16[3,64,1024]{2,1,0:T(8,128)(2,1)S(1)}, bf16[3,64,1024]{2,1,0:T(8,128)(2,1)S(1)}, u32[]{:S(2)}, u32[]{:S(2)}) collective-permute-start(bf16[3,64,1024]{2,1,0:T(8,128)(2,1)S(1)} %pad_maximum_fusion), channel_id=1, source_target_pairs={{0,2},{1,3},{2,0},{3,1},{4,6},{5,7},{6,4},{7,5},{8,10},{9,11},{10,... | collective-permute-start | bytes 1179656 | tf_op jit(solution)/shard_map/weights/ppermute | solution.py:31
  9.6 3.1 %collective-permute-start.2 = (bf16[3,64,1024]{2,1,0:T(8,128)(2,1)S(1)}, bf16[3,64,1024]{2,1,0:T(8,128)(2,1)S(1)}, u32[]{:S(2)}, u32[]{:S(2)}) collective-permute-start(bf16[3,64,1024]{2,1,0:T(8,128)(2,1)S(1)} %pad_maximum_fusion), channel_id=1, source_target_pairs={{0,3},{1,0},{2,1},{3,2},{4,7},{5,4},{6,5},{7,6},{8,11},{9,8},{10,9... | collective-permute-start | bytes 1179656 | tf_op jit(solution)/shard_map/weights/ppermute | solution.py:31
  12.7 0.7 fusion.29
  13.4 0.1 fusion.30
  13.5 0.7 select_reduce_fusion.2
  14.2 0.7 fusion.33
  14.9 0.3 fusion.12
  15.2 0.2 copy.41
  15.4 0.2 copy.40
  15.6 0.2 convolution_convert_fusion.1
  15.8 0.2 convolution_convert_fusion.2
  16.0 0.0 copy-start.5
  16.0 0.8 pad_maximum_fusion.1
  16.7 16.8 %all-to-all-start = ((bf16[32,16,128]{2,1,0:T(8,128)(2,1)}), bf16[32,16,128]{2,1,0:T(8,128)(2,1)S(1)}, u32[]{:S(2)}, u32[]{:S(2)}) async-start(bf16[32,16,128]{2,1,0:T(8,128)(2,1)} %pad_maximum_fusion.1), calls=%async_computation | async-start | bytes 262144 | tf_op jit(solution)/shard_map/all_to_all | solution.py:61
  33.5 0.2 broadcast_in_dim.72
  33.8 0.1 mul.49
  33.9 0.0 collective-permute-done
  33.9 1.0 bitcast_dynamic-update-slice_fusion.2
  34.9 0.0 collective-permute-done.1
  35.0 14.5 %all-to-all-done = bf16[32,16,128]{2,1,0:T(8,128)(2,1)S(1)} async-done(((bf16[32,16,128]{2,1,0:T(8,128)(2,1)}), bf16[32,16,128]{2,1,0:T(8,128)(2,1)S(1)}, u32[]{:S(2)}, u32[]{:S(2)}) %all-to-all-start) | async-done | bytes 131104 | tf_op jit(solution)/shard_map/all_to_all | solution.py:61
  49.5 0.1 copy.42
  49.7 0.9 broadcast_in_dim.78
  50.6 4.3 %all-to-all-start.1 = ((bf16[16,128,128]{1,2,0:T(8,128)(2,1)}), bf16[16,128,128]{1,2,0:T(8,128)(2,1)S(1)}, u32[]{:S(2)}, u32[]{:S(2)}) async-start(bf16[16,128,128]{1,2,0:T(8,128)(2,1)} %bitcast.21), calls=%async_computation.1 | async-start | bytes 1048576 | tf_op jit(solution)/shard_map/all_to_all | solution.py:65
  55.0 0.9 fusion.35
  55.9 10.0 %all-to-all-done.1 = bf16[16,128,128]{1,2,0:T(8,128)(2,1)S(1)} async-done(((bf16[16,128,128]{1,2,0:T(8,128)(2,1)}), bf16[16,128,128]{1,2,0:T(8,128)(2,1)S(1)}, u32[]{:S(2)}, u32[]{:S(2)}) %all-to-all-start.1) | async-done | bytes 524320 | tf_op jit(solution)/shard_map/all_to_all | solution.py:65
  65.9 0.2 fusion.7
  66.1 0.2 fusion.9
  66.3 0.5 copy.43
  66.9 0.3 convolution_minimum_fusion
  67.2 0.3 fusion.3
  67.5 10.5 %all_to_all.25 = bf16[4,256,256]{2,1,0:T(8,128)(2,1)S(1)} all-to-all(bf16[4,256,256]{2,1,0:T(8,128)(2,1)S(1)} %broadcast_in_dim.79), channel_id=1, replica_groups=mesh['ep'=32,'ty'=4,'tx'=4] {'ty'}, dimensions={0} | all-to-all | bytes 1048576 | tf_op jit(solution)/shard_map/all_to_all | solution.py:77
  78.1 0.3 convolution_convert_fusion
  78.4 8.0 %all_to_all.26 = bf16[4,64,256]{2,1,0:T(8,128)(2,1)S(1)} all-to-all(bf16[4,64,256]{2,1,0:T(8,128)(2,1)S(1)} %bitcast.82), channel_id=1, replica_groups=mesh['ep'=32,'ty'=4,'tx'=4] {'tx'}, dimensions={0} | all-to-all | bytes 262144 | tf_op jit(solution)/shard_map/all_to_all | solution.py:79
  86.4 0.2 copy.44
  86.6 0.3 copy.45
  86.9 0.8 reshape.92
  87.7 6.8 %all-to-all-start.4 = ((bf16[32,16,128]{2,1,0:T(8,128)(2,1)}), bf16[32,16,128]{2,1,0:T(8,128)(2,1)S(1)}, u32[]{:S(2)}, u32[]{:S(2)}) async-start(bf16[32,16,128]{2,1,0:T(8,128)(2,1)} %reshape.92), calls=%async_computation.4 | async-start | bytes 262144 | tf_op jit(solution)/shard_map/all_to_all | solution.py:83
  94.5 0.4 select_reduce_fusion
  94.9 15.8 %all-to-all-done.4 = bf16[32,16,128]{2,1,0:T(8,128)(2,1)S(1)} async-done(((bf16[32,16,128]{2,1,0:T(8,128)(2,1)}), bf16[32,16,128]{2,1,0:T(8,128)(2,1)S(1)}, u32[]{:S(2)}, u32[]{:S(2)}) %all-to-all-start.4) | async-done | bytes 131104 | tf_op jit(solution)/shard_map/all_to_all | solution.py:83
  110.6 0.2 fusion.24
  110.9 0.2 convolution_add_fusion.2
  111.1 0.3 convolution_add_fusion.1
  111.4 0.9 fusion.4
  (18 shorter events, 0.2 us)
Async XLA Ops:
  0.0 15.6 %copy-start = (bf16[128,64]{0,1:T(8,128)(2,1)S(1)}, bf16[128,64]{0,1:T(8,128)(2,1)}, u32[]{:S(2)}) copy-start(bf16[128,64]{0,1:T(8,128)(2,1)} %param.7) | copy-start | bytes 49156
  1.1 32.6 %copy-start.2 = (bf16[1,1024,64]{1,2,0:T(8,128)(2,1)S(1)}, bf16[1,1024,64]{1,2,0:T(8,128)(2,1)}, u32[]{:S(2)}) copy-start(bf16[1,1024,64]{1,2,0:T(8,128)(2,1)} %param.11) | copy-start | bytes 393220
  1.1 32.6 %copy-start.3 = (bf16[1,1024,64]{1,2,0:T(8,128)(2,1)S(1)}, bf16[1,1024,64]{1,2,0:T(8,128)(2,1)}, u32[]{:S(2)}) copy-start(bf16[1,1024,64]{1,2,0:T(8,128)(2,1)} %param.10) | copy-start | bytes 393220
  1.1 32.6 %copy-start.4 = (bf16[1,1024,64]{1,2,0:T(8,128)(2,1)S(1)}, bf16[1,1024,64]{1,2,0:T(8,128)(2,1)}, u32[]{:S(2)}) copy-start(bf16[1,1024,64]{1,2,0:T(8,128)(2,1)} %param.9) | copy-start | bytes 393220
  1.1 32.8 %collective-permute-start = (bf16[3,64,1024]{2,1,0:T(8,128)(2,1)S(1)}, bf16[3,64,1024]{2,1,0:T(8,128)(2,1)}, u32[]{:S(2)}, u32[]{:S(2)}) collective-permute-start(bf16[3,64,1024]{2,1,0:T(8,128)(2,1)S(1)} %pad_maximum_fusion), channel_id=1, source_target_pairs={{0,1},{1,2},{2,3},{3,0},{4,5},{5,6},{6,7},{7,4},{8,9},{9,10},{10,1... | collective-permute-start | bytes 1179656 | tf_op jit(solution)/shard_map/weights/ppermute | solution.py:31
  5.2 29.7 %collective-permute-start.1 = (bf16[3,64,1024]{2,1,0:T(8,128)(2,1)S(1)}, bf16[3,64,1024]{2,1,0:T(8,128)(2,1)S(1)}, u32[]{:S(2)}, u32[]{:S(2)}) collective-permute-start(bf16[3,64,1024]{2,1,0:T(8,128)(2,1)S(1)} %pad_maximum_fusion), channel_id=1, source_target_pairs={{0,2},{1,3},{2,0},{3,1},{4,6},{5,7},{6,4},{7,5},{8,10},{9,11},{10,... | collective-permute-start | bytes 1179656 | tf_op jit(solution)/shard_map/weights/ppermute | solution.py:31
  9.6 45.3 %collective-permute-start.2 = (bf16[3,64,1024]{2,1,0:T(8,128)(2,1)S(1)}, bf16[3,64,1024]{2,1,0:T(8,128)(2,1)S(1)}, u32[]{:S(2)}, u32[]{:S(2)}) collective-permute-start(bf16[3,64,1024]{2,1,0:T(8,128)(2,1)S(1)} %pad_maximum_fusion), channel_id=1, source_target_pairs={{0,3},{1,0},{2,1},{3,2},{4,7},{5,4},{6,5},{7,6},{8,11},{9,8},{10,9... | collective-permute-start | bytes 1179656 | tf_op jit(solution)/shard_map/weights/ppermute | solution.py:31
  16.0 17.9 %copy-start.5 = (f32[1024]{0:T(1024)S(1)}, f32[1024]{0:T(1024)}, u32[]{:S(2)}) copy-start(f32[1024]{0:T(1024)} %param.8) | copy-start | bytes 12292
  16.7 32.8 %all-to-all-start = ((bf16[32,16,128]{2,1,0:T(8,128)(2,1)}), bf16[32,16,128]{2,1,0:T(8,128)(2,1)S(1)}, u32[]{:S(2)}, u32[]{:S(2)}) async-start(bf16[32,16,128]{2,1,0:T(8,128)(2,1)} %pad_maximum_fusion.1), calls=%async_computation | async-start | bytes 262144 | tf_op jit(solution)/shard_map/all_to_all | solution.py:61
  50.6 15.3 %all-to-all-start.1 = ((bf16[16,128,128]{1,2,0:T(8,128)(2,1)}), bf16[16,128,128]{1,2,0:T(8,128)(2,1)S(1)}, u32[]{:S(2)}, u32[]{:S(2)}) async-start(bf16[16,128,128]{1,2,0:T(8,128)(2,1)} %bitcast.21), calls=%async_computation.1 | async-start | bytes 1048576 | tf_op jit(solution)/shard_map/all_to_all | solution.py:65
  55.9 11.0 %copy-start.1 = (bf16[4,1,64,1024]{3,2,1,0:T(8,128)(2,1)S(1)}, bf16[4,1,64,1024]{3,2,1,0:T(8,128)(2,1)}, u32[]{:S(2)}) copy-start(bf16[4,1,64,1024]{3,2,1,0:T(8,128)(2,1)} %get-tuple-element.12) | copy-start | bytes 1572868
  78.1 16.4 %copy-start.6 = (f32[128,4]{0,1:T(4,128)S(1)}, f32[128,4]{0,1:T(4,128)}, u32[]{:S(2)}) copy-start(f32[128,4]{0,1:T(4,128)} %param.13) | copy-start | bytes 6148
  87.7 23.0 %all-to-all-start.4 = ((bf16[32,16,128]{2,1,0:T(8,128)(2,1)}), bf16[32,16,128]{2,1,0:T(8,128)(2,1)S(1)}, u32[]{:S(2)}, u32[]{:S(2)}) async-start(bf16[32,16,128]{2,1,0:T(8,128)(2,1)} %reshape.92), calls=%async_computation.4 | async-start | bytes 262144 | tf_op jit(solution)/shard_map/all_to_all | solution.py:83

commit v3 on v2

v3 whole, which is shorter than its diff:
```python
import functools

import jax
import jax.numpy as jnp
from jax import lax
from jax.experimental import pallas as pl
from jax.experimental.pallas import tpu as pltpu
from jax.sharding import Mesh
from jax.sharding import PartitionSpec as P


EP, TY, TX = "ep", "ty", "tx"
TP = (TY, TX)
EPSILON = 1e-06
ALPHA = 1.702
LIMIT = 7.0
BF16, F32, I32 = jnp.bfloat16, jnp.float32, jnp.int32
NT = (((1,), (1,)), ((), ()))


def iota(shape, dim):
    return lax.broadcasted_iota(I32, shape, dim)


def dot(a, b):
    return jnp.dot(a, b, preferred_element_type=F32)


def dot_nt(a, b):
    return lax.dot_general(a, b, NT, preferred_element_type=F32)


def ones_where(mask):
    return jnp.where(mask, 1.0, 0.0).astype(BF16)


def swapped(count, middle, inner):
    outer = count // (middle * inner)
    to, source = iota((count, count), 0), iota((count, count), 1)
    m, o, i = to // (outer * inner), (to // inner) % outer, to % inner
    return ones_where(source == (o * middle + m) * inner + i)


def halves(first, second):
    wide = first.shape[1] // 2
    left = iota(first.shape, 1) < wide
    return (
        jnp.where(left, first, pltpu.roll(second, wide, 1)),
        jnp.where(left, pltpu.roll(first, wide, 1), second),
    )


def prep_kernel(experts, ids_ref, tokens_ref, sent_ref, place_ref):
    top, toks = ids_ref.shape
    count, _ = sent_ref.shape
    half = count // experts
    ids = ids_ref[...]
    expert = iota((experts, toks), 0)
    picks = [expert == ids[k : k + 1] for k in range(top)]
    named = picks[0]
    for pick in picks[1:]:
        named = named | pick
    earlier = ones_where(iota((toks, toks), 0) < iota((toks, toks), 1))
    before = dot(ones_where(named), earlier)
    lane = iota((2 * count, toks), 0)
    hit = None
    for k in range(top):
        slot = jnp.sum(jnp.where(picks[k], before, 0.0), axis=0, keepdims=True).astype(I32)
        high = jnp.where(slot >= half, 1, 0)
        place = ids[k : k + 1] * half + slot - half * high + count * high
        place_ref[k : k + 1] = place
        hit = (lane == place) if hit is None else hit | (lane == place)
    select = ones_where(hit)
    tokens = tokens_ref[...].astype(F32)
    zero = jnp.zeros_like(tokens)
    both = jnp.concatenate(
        [jnp.concatenate([tokens, zero], 1), jnp.concatenate([zero, tokens], 1)], 0
    ).astype(BF16)
    both_select = jnp.concatenate([select[:count], select[count:]], 1)
    sent_ref[...] = dot_nt(both_select, both).astype(BF16)


def mix_kernel(place_ref, weight_ref, first_ref, rest_ref):
    count, toks = first_ref.shape
    lane = iota((count, toks), 0)
    mix = jnp.zeros((count, toks), F32)
    for k in range(place_ref.shape[0]):
        mix = mix + jnp.where(lane == place_ref[k : k + 1], weight_ref[k : k + 1], 0.0)
    first = mix.astype(BF16)
    first_ref[...] = first
    rest_ref[...] = (mix - first.astype(F32)).astype(BF16)


def spread_kernel(got_ref, out_ref):
    count = got_ref.shape[0]
    copies, groups, group, _ = out_ref.shape
    order = swapped(count, groups, 4)
    moved = dot(order, got_ref[...]).astype(BF16)
    for g in range(groups):
        for c in range(copies):
            out_ref[c, g] = moved[g * group : (g + 1) * group]


def up_kernel(rows_ref, gain_ref, weights_ref, out_ref, whole, normed):
    pieces, group, wide = rows_ref.shape
    full = normed.shape[1]
    squares = [jnp.zeros((group, wide), F32) for _ in range(2)]
    for j in range(pieces // 2):
        pair = halves(rows_ref[2 * j].astype(F32), rows_ref[2 * j + 1].astype(F32))
        for h in range(2):
            whole[h * group : (h + 1) * group, j * wide : (j + 1) * wide] = pair[h]
            squares[h] = squares[h] + pair[h] * pair[h]
    for h in range(2):
        mean = jnp.sum(squares[h], axis=1, keepdims=True) / full
        inverse = lax.rsqrt(mean + EPSILON)
        rows = slice(h * group, (h + 1) * group)
        normed[rows] = (whole[rows] * inverse * gain_ref[...]).astype(BF16)
    nx, _, units, _ = weights_ref.shape
    w_gate = weights_ref[:, 0].reshape(nx * units, full)
    w_up = weights_ref[:, 1].reshape(nx * units, full)
    gate = jnp.minimum(dot_nt(normed[...], w_gate), LIMIT)
    up = jnp.clip(dot_nt(normed[...], w_up), -LIMIT, LIMIT)
    hidden = ((up + 1.0) * gate * jax.nn.sigmoid(ALPHA * gate)).astype(BF16)
    for c in range(out_ref.shape[0]):
        out_ref[c] = hidden


def down_kernel(hidden_ref, weights_ref, out_ref):
    ny, rows, units = hidden_ref.shape
    nx, _, width, full = weights_ref.shape
    w_down = weights_ref[:, 2].reshape(nx * width, full)
    total = dot_nt(hidden_ref[0], w_down[:, :units])
    for y in range(1, ny):
        total = total + dot_nt(hidden_ref[y], w_down[:, y * units : (y + 1) * units])
    group = rows // 2
    pieces = []
    for j in range(nx // 2):
        lanes = slice(2 * j * width, 2 * (j + 1) * width)
        pieces += halves(total[:group, lanes], total[group:, lanes])
    stacked = jnp.concatenate(pieces, 0).astype(BF16)
    order = swapped(stacked.shape[0], stacked.shape[0] // (nx * 4), 4)
    out_ref[...] = dot(order, stacked).astype(BF16)


def combine_kernel(back_ref, first_ref, rest_ref, out_ref):
    count = back_ref.shape[0]
    width = out_ref.shape[0]
    back = back_ref[...].astype(F32).T.astype(BF16)
    total = jnp.zeros(out_ref.shape, F32)
    for h in range(2):
        piece = back[h * width : (h + 1) * width]
        for part in (first_ref, rest_ref):
            total = total + dot(piece, part[h * count : (h + 1) * count])
    out_ref[...] = total.astype(BF16)


def call(kernel, out_shapes, *args, flops=1 << 24, scratch=()):
    single = not isinstance(out_shapes, list)
    specs = [pl.BlockSpec(memory_space=pltpu.VMEM)] * len(args)
    outs = [out_shapes] if single else out_shapes
    out_specs = [pl.BlockSpec(memory_space=pltpu.VMEM)] * len(outs)
    return pl.pallas_call(
        kernel,
        out_shape=out_shapes,
        in_specs=specs,
        out_specs=out_specs[0] if single else out_specs,
        scratch_shapes=list(scratch),
        cost_estimate=pl.CostEstimate(flops=flops, bytes_accessed=1 << 20, transcendentals=0),
        compiler_params=pltpu.CompilerParams(vmem_limit_bytes=16 << 20),
    )(*args)


def gathered(shard, axis):
    count = lax.axis_size(axis)
    me = lax.axis_index(axis)
    whole = jnp.zeros((count,) + shard.shape, shard.dtype)
    whole = lax.dynamic_update_slice_in_dim(whole, shard[None], me, 0)
    for hop in range(1, count):
        piece = lax.ppermute(shard, axis, [(i, (i + hop) % count) for i in range(count)])
        source = lax.rem(me + (count - hop), count)
        whole = lax.dynamic_update_slice_in_dim(whole, piece[None], source, 0)
    return whole


def body(tokens, norm_gain, gate_weight, up_weight, down_weight, expert_ids, route_weight):
    tok_rows, top = expert_ids.shape
    width = tokens.shape[1]
    full = norm_gain.shape[0]
    ep, ny, nx = lax.axis_size(EP), lax.axis_size(TY), lax.axis_size(TX)
    tp = ny * nx
    units = gate_weight.shape[2]
    half = tok_rows * top // ep
    count, wide = ep * half, 2 * width
    group = count // nx
    shape = jax.ShapeDtypeStruct

    sent, place = call(
        functools.partial(prep_kernel, ep),
        [shape((count, wide), BF16), shape((top, tok_rows), I32)],
        expert_ids.T,
        tokens.T,
    )
    got = lax.all_to_all(sent.reshape(ep, half, wide), EP, 0, 0, tiled=True)

    shard = jnp.stack([w[0].T for w in (gate_weight, up_weight, down_weight)])
    weights = gathered(shard, TX)

    spread = call(spread_kernel, shape((ny, nx, group, wide), BF16), got.reshape(count, wide))
    rows = lax.all_to_all(spread.reshape(tp, group, wide), TP, 0, 0, tiled=True)
    hidden = call(
        up_kernel,
        shape((ny, 2 * group, nx * units), BF16),
        rows,
        norm_gain.astype(F32).reshape(1, full),
        weights,
        flops=1 << 28,
        scratch=(pltpu.VMEM((2 * group, full), F32), pltpu.VMEM((2 * group, full), BF16)),
    )
    hidden = lax.all_to_all(hidden, TY, 0, 0, tiled=True)
    out = call(down_kernel, shape((count, wide), BF16), hidden, weights, flops=1 << 27)

    back = lax.all_to_all(out.reshape(ep * nx, half // nx, wide), (EP, TX), 0, 0, tiled=True)
    first, rest = call(
        mix_kernel,
        [shape((2 * count, tok_rows), BF16)] * 2,
        place,
        route_weight.astype(F32).T,
    )
    combined = call(
        combine_kernel, shape((width, tok_rows), BF16), back.reshape(count, wide), first, rest
    )
    return combined.T


def solution(mesh):
    devices = mesh.devices.reshape(mesh.shape["ep"], 4, 4)
    split = Mesh(devices, (EP, TY, TX))
    in_specs = (
        P(EP, TP),
        P(),
        P(EP, None, TP),
        P(EP, None, TP),
        P(EP, None, TP),
        P(EP, None),
        P(EP, None),
    )
    return jax.shard_map(body, mesh=split, in_specs=in_specs, out_specs=P(EP, TP), check_vma=False)
```

time: 113 us -> 103 us (0.912)
  starting transfers between devices: 39.4 us -> 52.6 us
  waiting for transfers between devices: 40.3 us -> 30.6 us
  blocking collectives: 18.6 us -> 9.33 us
  Pallas kernels: 0 us -> 5.84 us
  other arithmetic: 5.13 us -> 1.12 us
  matrix products: 3.01 us -> 0 us
  local copies, waits for them, and re-layouts: 5.5 us -> 2.7 us
    all_to_all x3, starting transfers between devices: 27.9 us -> 42.1 us  [the longest x1 18.5 us: body(): lax.all_to_all(out.reshape(ep * nx, half // nx, wide), (EP, TX), 0, 0, ti...]
    all_to_all x3, waiting for transfers between devices: 40.3 us -> 30.2 us  [the longest x1 17.8 us: body(): lax.all_to_all(out.reshape(ep * nx, half // nx, wide), (EP, TX), 0, 0, ti...]
    all_to_all x2 -> x1, blocking collectives: 18.6 us -> 9.33 us  [body(): hidden = lax.all_to_all(hidden, TY, 0, 0, tiled=True)]
    pallas_call x0 -> x6, Pallas kernels: none -> 5.84 us  [call(): pl.pallas_call(kernel, out_shape=out_shapes, in_specs=specs, out_specs=ou...]
    dot_general x10 -> x0, matrix products: 3.01 us -> none  [the longest x4 1.61 us: body(): jnp.dot(part.astype(BF16), piece, preferred_element_type=F32)]
    unnamed x14, local copies, waits for them, and re-layouts: 0.04 us -> 1.42 us
    reduce_sum x3 -> x0, other arithmetic: 1.29 us -> none  [the longest x1 0.72 us: routed_to(): jnp.sum(jnp.where(picks, before[:, None, :], 0.0), axis=2).astype(jnp.int32)]
  transfers between devices with their start and end apart: 6 -> 6, of which waited for: 3 -> 4; matrix products, arithmetic and copies ran while one was open for 7% -> 2% of each run, Pallas kernels for 0% -> 1%
where the time goes in v3:
time: 103 us; the launch traced here: 102 us
  starting transfers between devices  52.6 us (51%)
  waiting for transfers between devices  30.6 us (30%)
  blocking collectives  9.33 us (9%)
  Pallas kernels  5.84 us (6%)
  local copies, waits for them, and re-layouts  2.7 us (3%)
  other arithmetic  1.12 us (1%)
    all_to_all x1, starting transfers between devices, body(): lax.all_to_all(out.reshape(ep * nx, half // nx, wide), (EP, TX), 0, 0, ti...  18.5 us
    all_to_all x1, waiting for transfers between devices, body(): lax.all_to_all(out.reshape(ep * nx, half // nx, wide), (EP, TX), 0, 0, ti...  17.8 us
    all_to_all x1, starting transfers between devices, body(): got = lax.all_to_all(sent.reshape(ep, half, wide), EP, 0, 0, tiled=True)  16.7 us
    ppermute x3, starting transfers between devices, gathered(): lax.ppermute(shard, axis, [(i, (i + hop) % count) for i in range(count)])  10.5 us
    all_to_all x1, blocking collectives, body(): hidden = lax.all_to_all(hidden, TY, 0, 0, tiled=True)  9.33 us
    all_to_all x1, waiting for transfers between devices, body(): rows = lax.all_to_all(spread.reshape(tp, group, wide), TP, 0, 0, tiled=True)  8.48 us
    all_to_all x1, starting transfers between devices, body(): rows = lax.all_to_all(spread.reshape(tp, group, wide), TP, 0, 0, tiled=True)  6.89 us
    pallas_call x6, Pallas kernels, call(): pl.pallas_call(kernel, out_shape=out_shapes, in_specs=specs, out_specs=ou...  5.84 us
  transfers between devices with their start and end apart: 6, of which 4 were waited for; matrix products, arithmetic and copies ran while one was open for 2% of the time, Pallas kernels for 1%

profile of v3, /device:TPU:1, one launch (start us, length us, event | category | flops | bytes accessed | tf_op | source)
XLA Modules:
  0.0 102.4 jit_solution(9983001757350492813)
XLA Ops:
  0.0 0.0 copy-start.1
  0.0 0.7 copy-done.1
  0.7 0.0 copy-start.2
  0.7 0.7 copy-done.2
  1.4 0.0 copy-start.4
  1.4 0.0 copy-start.5
  1.4 0.0 copy-start.6
  1.4 1.2 %shard_map.73 = (bf16[512,128]{1,0:T(8,128)(2,1)}, s32[4,128]{1,0:T(4,128)S(1)}) custom-call(s32[4,128]{1,0:T(4,128)S(1)} %bitcast.37, bf16[64,128]{1,0:T(8,128)(2,1)S(1)} %bitcast.36), custom_call_target="tpu_custom_call" | custom-call | flops 16777216 | bytes 1048576 | tf_op jit(solution)/shard_map/pallas_call | solution.py:162
  2.6 16.7 %all-to-all-start = ((bf16[32,16,128]{2,1,0:T(8,128)(2,1)}), bf16[32,16,128]{2,1,0:T(8,128)(2,1)S(1)}, u32[]{:S(2)}, u32[]{:S(2)}) async-start(bf16[32,16,128]{2,1,0:T(8,128)(2,1)} %bitcast.2), calls=%async_computation | async-start | bytes 262144 | tf_op jit(solution)/shard_map/all_to_all | solution.py:203
  19.3 1.1 %pad_maximum_fusion = bf16[3,64,1024]{2,1,0:T(8,128)(2,1)S(1)} fusion(bf16[1,64,1024]{2,1,0:T(8,128)(2,1)} %bitcast.39, bf16[1,64,1024]{2,1,0:T(8,128)(2,1)} %bitcast.41, bf16[1,64,1024]{2,1,0:T(8,128)(2,1)} %bitcast.43), kind=kLoop, calls=%fused_computation | loop fusion | flops 393216 | bytes 786432 | tf_op jit(solution)/shard_map/stack | solution.py:205
  20.4 3.1 %collective-permute-start = (bf16[3,64,1024]{2,1,0:T(8,128)(2,1)S(1)}, bf16[3,64,1024]{2,1,0:T(8,128)(2,1)}, u32[]{:S(2)}, u32[]{:S(2)}) collective-permute-start(bf16[3,64,1024]{2,1,0:T(8,128)(2,1)S(1)} %pad_maximum_fusion), channel_id=1, source_target_pairs={{0,1},{1,2},{2,3},{3,0},{4,5},{5,6},{6,7},{7,4},{8,9},{9,10},{10,1... | collective-permute-start | bytes 1179656 | tf_op jit(solution)/shard_map/ppermute | solution.py:179
  23.5 4.4 %collective-permute-start.1 = (bf16[3,64,1024]{2,1,0:T(8,128)(2,1)S(1)}, bf16[3,64,1024]{2,1,0:T(8,128)(2,1)S(1)}, u32[]{:S(2)}, u32[]{:S(2)}) collective-permute-start(bf16[3,64,1024]{2,1,0:T(8,128)(2,1)S(1)} %pad_maximum_fusion), channel_id=1, source_target_pairs={{0,2},{1,3},{2,0},{3,1},{4,6},{5,7},{6,4},{7,5},{8,10},{9,11},{10,... | collective-permute-start | bytes 1179656 | tf_op jit(solution)/shard_map/ppermute | solution.py:179
  27.9 3.1 %collective-permute-start.2 = (bf16[3,64,1024]{2,1,0:T(8,128)(2,1)S(1)}, bf16[3,64,1024]{2,1,0:T(8,128)(2,1)S(1)}, u32[]{:S(2)}, u32[]{:S(2)}) collective-permute-start(bf16[3,64,1024]{2,1,0:T(8,128)(2,1)S(1)} %pad_maximum_fusion), channel_id=1, source_target_pairs={{0,3},{1,0},{2,1},{3,2},{4,7},{5,4},{6,5},{7,6},{8,11},{9,8},{10,9... | collective-permute-start | bytes 1179656 | tf_op jit(solution)/shard_map/ppermute | solution.py:179
  31.0 0.2 broadcast_in_dim.15
  31.2 0.0 copy-done.4
  31.2 0.0 copy-done.5
  31.2 0.0 copy-done.6
  31.3 3.9 %all-to-all-done = bf16[32,16,128]{2,1,0:T(8,128)(2,1)S(1)} async-done(((bf16[32,16,128]{2,1,0:T(8,128)(2,1)}), bf16[32,16,128]{2,1,0:T(8,128)(2,1)S(1)}, u32[]{:S(2)}, u32[]{:S(2)}) %all-to-all-start) | async-done | bytes 131104 | tf_op jit(solution)/shard_map/all_to_all | solution.py:203
  35.2 1.1 %shard_map.74 = bf16[4,4,128,128]{3,2,1,0:T(8,128)(2,1)} custom-call(bf16[512,128]{1,0:T(8,128)(2,1)S(1)} %bitcast.33), custom_call_target="tpu_custom_call" | custom-call | flops 16777216 | bytes 1048576 | tf_op jit(solution)/shard_map/pallas_call | solution.py:162
  36.3 0.0 copy-start
  36.3 6.9 %all-to-all-start.1 = ((bf16[16,128,128]{2,1,0:T(8,128)(2,1)}), bf16[16,128,128]{2,1,0:T(8,128)(2,1)S(1)}, u32[]{:S(2)}, u32[]{:S(2)}) async-start(bf16[16,128,128]{2,1,0:T(8,128)(2,1)} %bitcast.4), calls=%async_computation.1 | async-start | bytes 1048576 | tf_op jit(solution)/shard_map/all_to_all | solution.py:209
  43.2 0.0 collective-permute-done
  43.2 1.0 %bitcast_dynamic-update-slice_fusion.2 = bf16[4,3,64,1024]{3,2,1,0:T(8,128)(2,1)S(1)} fusion(bf16[4,3,64,1024]{3,2,1,0:T(8,128)(2,1)S(1)} %bitcast_dynamic-update-slice_fusion.3, s32[]{:T(128)S(6)} %select_n.13, bf16[3,64,1024]{2,1,0:T(8,128)(2,1)} %collective-permute-done), kind=kLoop, calls=%fused_computation.3 | loop fusion | bytes 786436 | tf_op jit(solution)/shard_map/dynamic_update_slice | solution.py:181
  44.2 0.0 collective-permute-done.1
  44.3 0.4 collective-permute-done.2
  44.7 8.5 %all-to-all-done.1.rows_ref = bf16[16,128,128]{2,1,0:T(8,128)(2,1)S(1)} async-done(((bf16[16,128,128]{2,1,0:T(8,128)(2,1)}), bf16[16,128,128]{2,1,0:T(8,128)(2,1)S(1)}, u32[]{:S(2)}, u32[]{:S(2)}) %all-to-all-start.1) | async-done | bytes 524320 | tf_op jit(solution)/shard_map/all_to_all | solution.py:209
  53.1 0.0 copy-done
  53.1 0.9 shard_map.75
  54.0 0.0 copy-start.3
  54.0 9.3 %all_to_all.20.hidden_ref = bf16[4,256,256]{2,1,0:T(8,128)(2,1)S(1)} all-to-all(bf16[4,256,256]{2,1,0:T(8,128)(2,1)S(1)} %shard_map.75), channel_id=1, replica_groups=mesh['ep'=32,'ty'=4,'tx'=4] {'ty'}, dimensions={0} | all-to-all | bytes 1048576 | tf_op jit(solution)/shard_map/all_to_all | solution.py:219
  63.4 1.6 %shard_map.76 = bf16[512,128]{1,0:T(8,128)(2,1)} custom-call(bf16[4,256,256]{2,1,0:T(8,128)(2,1)S(1)} %all_to_all.20.hidden_ref, bf16[4,3,64,1024]{3,2,1,0:T(8,128)(2,1)S(1)} %bitcast_dynamic-update-slice_fusion.weights_ref), custom_call_target="tpu_custom_call" | custom-call | flops 134217728 | bytes 1048576 | tf_op jit(solution)/shard_map/pallas_call | solution.py:162
  64.9 18.5 %all-to-all-start.3 = ((bf16[128,4,128]{2,1,0:T(4,128)(2,1)}), bf16[128,4,128]{2,1,0:T(4,128)(2,1)S(1)}, u32[]{:S(2)}, u32[]{:S(2)}) async-start(bf16[128,4,128]{2,1,0:T(4,128)(2,1)} %bitcast.19), calls=%async_computation.3 | async-start | bytes 262144 | tf_op jit(solution)/shard_map/all_to_all | solution.py:222
  83.4 0.0 copy-done.3
  83.4 0.3 shard_map.77
  83.7 17.8 %all-to-all-done.3 = bf16[128,4,128]{2,1,0:T(4,128)(2,1)S(1)} async-done(((bf16[128,4,128]{2,1,0:T(4,128)(2,1)}), bf16[128,4,128]{2,1,0:T(4,128)(2,1)S(1)}, u32[]{:S(2)}, u32[]{:S(2)}) %all-to-all-start.3) | async-done | bytes 131104 | tf_op jit(solution)/shard_map/all_to_all | solution.py:222
  101.5 0.9 shard_map.78
  (3 shorter events, 0.1 us)
Async XLA Ops:
  0.0 0.7 copy-start.1
  0.7 0.7 copy-start.2
  1.4 29.8 %copy-start.4 = (bf16[1,1024,64]{1,2,0:T(8,128)(2,1)S(1)}, bf16[1,1024,64]{1,2,0:T(8,128)(2,1)}, u32[]{:S(2)}) copy-start(bf16[1,1024,64]{1,2,0:T(8,128)(2,1)} %param.11) | copy-start | bytes 393220
  1.4 29.8 %copy-start.5 = (bf16[1,1024,64]{1,2,0:T(8,128)(2,1)S(1)}, bf16[1,1024,64]{1,2,0:T(8,128)(2,1)}, u32[]{:S(2)}) copy-start(bf16[1,1024,64]{1,2,0:T(8,128)(2,1)} %param.10) | copy-start | bytes 393220
  1.4 29.8 %copy-start.6 = (bf16[1,1024,64]{1,2,0:T(8,128)(2,1)S(1)}, bf16[1,1024,64]{1,2,0:T(8,128)(2,1)}, u32[]{:S(2)}) copy-start(bf16[1,1024,64]{1,2,0:T(8,128)(2,1)} %param.9) | copy-start | bytes 393220
  2.6 32.6 %all-to-all-start = ((bf16[32,16,128]{2,1,0:T(8,128)(2,1)}), bf16[32,16,128]{2,1,0:T(8,128)(2,1)S(1)}, u32[]{:S(2)}, u32[]{:S(2)}) async-start(bf16[32,16,128]{2,1,0:T(8,128)(2,1)} %bitcast.2), calls=%async_computation | async-start | bytes 262144 | tf_op jit(solution)/shard_map/all_to_all | solution.py:203
  20.4 22.8 %collective-permute-start = (bf16[3,64,1024]{2,1,0:T(8,128)(2,1)S(1)}, bf16[3,64,1024]{2,1,0:T(8,128)(2,1)}, u32[]{:S(2)}, u32[]{:S(2)}) collective-permute-start(bf16[3,64,1024]{2,1,0:T(8,128)(2,1)S(1)} %pad_maximum_fusion), channel_id=1, source_target_pairs={{0,1},{1,2},{2,3},{3,0},{4,5},{5,6},{6,7},{7,4},{8,9},{9,10},{10,1... | collective-permute-start | bytes 1179656 | tf_op jit(solution)/shard_map/ppermute | solution.py:179
  23.5 20.7 %collective-permute-start.1 = (bf16[3,64,1024]{2,1,0:T(8,128)(2,1)S(1)}, bf16[3,64,1024]{2,1,0:T(8,128)(2,1)S(1)}, u32[]{:S(2)}, u32[]{:S(2)}) collective-permute-start(bf16[3,64,1024]{2,1,0:T(8,128)(2,1)S(1)} %pad_maximum_fusion), channel_id=1, source_target_pairs={{0,2},{1,3},{2,0},{3,1},{4,6},{5,7},{6,4},{7,5},{8,10},{9,11},{10,... | collective-permute-start | bytes 1179656 | tf_op jit(solution)/shard_map/ppermute | solution.py:179
  27.9 16.7 %collective-permute-start.2 = (bf16[3,64,1024]{2,1,0:T(8,128)(2,1)S(1)}, bf16[3,64,1024]{2,1,0:T(8,128)(2,1)S(1)}, u32[]{:S(2)}, u32[]{:S(2)}) collective-permute-start(bf16[3,64,1024]{2,1,0:T(8,128)(2,1)S(1)} %pad_maximum_fusion), channel_id=1, source_target_pairs={{0,3},{1,0},{2,1},{3,2},{4,7},{5,4},{6,5},{7,6},{8,11},{9,8},{10,9... | collective-permute-start | bytes 1179656 | tf_op jit(solution)/shard_map/ppermute | solution.py:179
  36.3 16.9 %copy-start = (f32[1024]{0:T(1024)S(1)}, f32[1024]{0:T(1024)}, u32[]{:S(2)}) copy-start(f32[1024]{0:T(1024)} %param.8) | copy-start | bytes 12292
  36.3 16.9 %all-to-all-start.1 = ((bf16[16,128,128]{2,1,0:T(8,128)(2,1)}), bf16[16,128,128]{2,1,0:T(8,128)(2,1)S(1)}, u32[]{:S(2)}, u32[]{:S(2)}) async-start(bf16[16,128,128]{2,1,0:T(8,128)(2,1)} %bitcast.4), calls=%async_computation.1 | async-start | bytes 1048576 | tf_op jit(solution)/shard_map/all_to_all | solution.py:209
  54.0 29.4 %copy-start.3 = (f32[128,4]{0,1:T(4,128)S(1)}, f32[128,4]{0,1:T(4,128)}, u32[]{:S(2)}) copy-start(f32[128,4]{0,1:T(4,128)} %param.13) | copy-start | bytes 6148
  64.9 36.6 %all-to-all-start.3 = ((bf16[128,4,128]{2,1,0:T(4,128)(2,1)}), bf16[128,4,128]{2,1,0:T(4,128)(2,1)S(1)}, u32[]{:S(2)}, u32[]{:S(2)}) async-start(bf16[128,4,128]{2,1,0:T(4,128)(2,1)} %bitcast.19), calls=%async_computation.3 | async-start | bytes 262144 | tf_op jit(solution)/shard_map/all_to_all | solution.py:222
